TPU v7x, 32 devices: a whole 2x2x4 slice. The times are simulated.
32 devices in a mesh: sp: 16 (over z, y, core), tp: 2 (over x).
Axes of the slice: x: 2, y: 2, z: 4, core: 2. Of those that a mesh axis runs over, the one named last changes fastest.
Arguments:
- tokens: bfloat16 [16384, 2048], P('sp'), may hold values from -6 to 6
- norm_gain: float32 [2048], replicated, may hold values from 0.1 to 1.9
- w_query: bfloat16 [2048, 512], P(None, 'tp'), may hold values from -0.79549513 to 0.79549513
- w_key: bfloat16 [2048, 128], P('sp'), may hold values from -0.79549513 to 0.79549513
- w_value: bfloat16 [2048, 128], P('sp'), may hold values from -0.125 to 0.125
- w_pool_in: bfloat16 [2048, 512], P(None, 'tp'), may hold values from -0.125 to 0.125
- sink_logit: float32 [8], P('tp'), may hold values from 3 to 7
- pool_scale: float32 [512], P('tp'), may hold values from 0.05 to 0.5
- w_out: bfloat16 [1024, 2048], P('tp', 'sp'), may hold values from -0.75 to 0.75
Outputs:
- mixed_out: bfloat16 [16384, 2048], P(('sp', 'tp'))
All inputs are finite; a program needn't handle non-finite values.
Results may differ from a plain program's by a relative error of at most 0.03.
The roundings to bfloat16 on the way count: a program that leaves them out, or rounds other values in their place, can miss the bound.
Values may be sent and summed in bfloat16 or wider, within the bound.
A program may use at most 64 MiB of HBM per device.

v0:
```python
import jax
import jax.numpy as jnp
from jax import lax
from jax.sharding import PartitionSpec as P

HEAD = 64
QH = 8
KVH = 2
POOL_CH = 128
WINDOW = 128
QB = 128
NEG_BIG = -1e30
POOL_SPANS = (2, 4, 8, 16)


def extended(block, sides, width):
    for axis, dim in sides:
        count = lax.axis_size(axis)
        forward = [(i, i + 1) for i in range(count - 1)]
        backward = [(target, source) for source, target in forward]
        low = lax.ppermute(
            lax.slice_in_dim(block, block.shape[dim] - width, None, axis=dim), axis, forward
        )
        high = lax.ppermute(lax.slice_in_dim(block, 0, width, axis=dim), axis, backward)
        block = jnp.concatenate([low, block, high], axis=dim)
    return block


def layer_normed(tokens, norm_gain):
    values = tokens.astype(jnp.float32)
    center = jnp.mean(values, axis=-1, keepdims=True)
    spread = jnp.mean(jnp.square(values - center), axis=-1, keepdims=True)
    return ((values - center) * lax.rsqrt(spread + 1e-06) * norm_gain).astype(jnp.bfloat16)


def rotate(values, positions):
    half = HEAD // 2
    inverse = 10000.0 ** (-jnp.arange(half, dtype=jnp.float32) / half)
    angles = positions[:, None] * inverse[None, :]
    cosine = jnp.cos(angles)[:, None, :]
    sine = jnp.sin(angles)[:, None, :]
    first = values[..., :half]
    second = values[..., half:]
    return jnp.concatenate(
        [first * cosine - second * sine, first * sine + second * cosine], axis=-1
    )


def body(tokens, norm_gain, w_query, w_key, w_value, w_pool_in, sink_logit, pool_scale, w_out):
    local_rows = tokens.shape[0]
    seq_total = local_rows * lax.axis_size("sp")
    offset = lax.axis_index("sp") * local_rows
    tp_place = lax.axis_index("tp")
    local_heads = w_query.shape[1] // HEAD
    local_pool = w_pool_in.shape[1]
    reach = POOL_SPANS[-1] // 2
    normed = layer_normed(tokens, norm_gain)
    positions = (offset + jnp.arange(local_rows)).astype(jnp.float32)
    query = rotate(
        jnp.dot(normed, w_query, preferred_element_type=jnp.float32).reshape(
            local_rows, local_heads, HEAD
        ),
        positions,
    ).astype(jnp.bfloat16)
    key_head = tp_place * local_heads // (QH // KVH)
    key_cols = lax.dynamic_slice_in_dim(w_key, key_head * HEAD, HEAD, 1)
    value_cols = lax.dynamic_slice_in_dim(w_value, key_head * HEAD, HEAD, 1)
    key_sum = jnp.dot(
        normed,
        lax.all_gather(key_cols, "sp", axis=0, tiled=True),
        preferred_element_type=jnp.float32,
    )
    value_sum = jnp.dot(
        normed,
        lax.all_gather(value_cols, "sp", axis=0, tiled=True),
        preferred_element_type=jnp.float32,
    )
    key = rotate(key_sum[:, None, :], positions)[:, 0, :].astype(jnp.bfloat16)
    value = value_sum.astype(jnp.bfloat16)
    key_value = jnp.concatenate([key, value], axis=1)
    pool_in = jnp.dot(normed, w_pool_in, preferred_element_type=jnp.float32).astype(jnp.bfloat16)
    widened = extended(jnp.concatenate([key_value, pool_in], axis=1), (("sp", 0),), WINDOW)
    kv_wide = widened[:, : 2 * HEAD]
    pool_wide = widened[WINDOW - reach : WINDOW + local_rows + reach, 2 * HEAD :]
    span = QB + 2 * WINDOW
    sink_here = sink_logit[:, None, None]
    results = []
    for block in range(local_rows // QB):
        queries = query[block * QB : (block + 1) * QB]
        keys = kv_wide[block * QB : block * QB + span, :HEAD]
        values = kv_wide[block * QB : block * QB + span, HEAD:]
        scores = jnp.einsum(
            "ihd,jd->hij", queries, keys, preferred_element_type=jnp.float32
        ) * HEAD ** (-0.5)
        query_pos = offset + block * QB + jnp.arange(QB)
        key_pos = offset + block * QB - WINDOW + jnp.arange(span)
        valid = (
            (jnp.abs(query_pos[:, None] - key_pos[None, :]) <= WINDOW)
            & (key_pos[None, :] >= 0)
            & (key_pos[None, :] < seq_total)
        )
        scores = jnp.where(valid, scores, NEG_BIG)
        highest = jnp.maximum(jnp.max(scores, axis=-1, keepdims=True), sink_here)
        expo = jnp.where(valid, jnp.exp(scores - highest), 0.0)
        total = jnp.sum(expo, axis=-1, keepdims=True) + jnp.exp(sink_here - highest)
        weights = (expo / total).astype(jnp.bfloat16)
        result = jnp.einsum("hij,jd->ihd", weights, values, preferred_element_type=jnp.float32)
        results.append(result.reshape(QB, local_heads * HEAD).astype(jnp.bfloat16))
    attended = jnp.concatenate(results, axis=0)
    pool_vals = pool_wide.astype(jnp.float32)
    window_sum = pool_vals
    global_pos = offset + jnp.arange(local_rows)
    channel = tp_place * local_pool + jnp.arange(local_pool)
    window_group = channel // POOL_CH
    measured = jnp.zeros((local_rows, local_pool), jnp.float32)
    stride = 1
    for index, width in enumerate(POOL_SPANS):
        window_sum = window_sum[:-stride] + window_sum[stride:]
        stride = width
        sums = window_sum[reach - width // 2 : reach - width // 2 + local_rows]
        counted = (
            jnp.minimum(global_pos + width // 2, seq_total)
            - jnp.maximum(global_pos - width // 2, 0)
        ).astype(jnp.float32)
        measured = measured + jnp.where(
            window_group[None, :] == index, sums / counted[:, None], 0.0
        )
    pooled = ((measured - pool_vals[reach : reach + local_rows]) * pool_scale).astype(jnp.bfloat16)
    attended_rows, pooled_rows = (
        lax.all_to_all(attended, "tp", split_axis=0, concat_axis=1, tiled=True),
        lax.all_to_all(pooled, "tp", split_axis=0, concat_axis=1, tiled=True),
    )
    joined = jnp.concatenate([attended_rows, pooled_rows], axis=1)
    out_rows_all = lax.all_gather(w_out, "tp", axis=0, tiled=True)
    projected = jnp.dot(
        joined,
        lax.all_gather(out_rows_all, "sp", axis=1, tiled=True),
        preferred_element_type=jnp.float32,
    )
    return projected.astype(jnp.bfloat16)


def solution(mesh):
    in_specs = (
        P("sp", None),
        P(),
        P(None, "tp"),
        P("sp", None),
        P("sp", None),
        P(None, "tp"),
        P("tp"),
        P("tp"),
        P("tp", "sp"),
    )
    out_specs = P(("sp", "tp"), None)
    return jax.shard_map(body, mesh=mesh, in_specs=in_specs, out_specs=out_specs, check_vma=False)
```

profile of v0, /device:TPU:0, one launch (start us, length us, event | category | flops | bytes accessed | tf_op | source)
XLA Modules:
  0.0 166.7 jit_solution(2030448479956947112)
XLA Ops:
  6.6 0.9 constant_dynamic-slice_fusion.1
  7.5 24.6 %all_gather.12 = bf16[2048,64]{1,0:T(8,128)(2,1)S(1)} all-gather(bf16[128,64]{1,0:T(8,128)(2,1)S(1)} %constant_dynamic-slice_fusion.1), channel_id=1, replica_groups=mesh['sp'=16,'tp'=2] {'sp'}, dimensions={0}, use_global_device_ids=true | all-gather | bytes 278528 | tf_op jit(solution)/shard_map/all_gather | solution.py:70
  32.1 3.0 %convert_reduce_fusion = f32[1024]{0:T(1024)S(1)} fusion(bf16[1024,2048]{1,0:T(8,128)(2,1)} %param.9), kind=kLoop, calls=%fused_computation.1 | loop fusion | flops 4193280 | bytes 4198400 | tf_op jit(solution)/shard_map/reduce_sum | solution.py:31
  35.5 1.2 fusion.2
  36.9 18.9 %all_gather.13 = bf16[2048,64]{1,0:T(8,128)(2,1)S(1)} all-gather(bf16[128,64]{1,0:T(8,128)(2,1)S(1)} %constant_dynamic-slice_fusion), channel_id=1, replica_groups=mesh['sp'=16,'tp'=2] {'sp'}, dimensions={0}, use_global_device_ids=true | all-gather | bytes 278528 | tf_op jit(solution)/shard_map/all_gather | solution.py:75
  55.8 3.0 %fusion.4 = bf16[1024,2048]{1,0:T(8,128)(2,1)S(1)} fusion(bf16[1024,2048]{1,0:T(8,128)(2,1)} %param.9, f32[2048]{0:T(1024)S(1)} %copy-done.53, f32[1024]{0:T(1024)S(1)} %add_rsqrt_fusion, f32[1024]{0:T(1024)S(1)} %broadcast_multiply_fusion), kind=kLoop, calls=%fused_computation.6 | loop fusion | flops 10485760 | bytes 8404992 | tf_op jit(solution)/shard_map/convert_element_type | solution.py:33
  58.8 1.4 convolution_bitcast_fusion
  60.2 1.4 convolution_convert_fusion.2
  61.6 1.3 convolution_convert_fusion.1
  63.6 1.3 collective-permute-start.1
  64.9 3.7 %collective-permute-start = (bf16[128,384]{0,1:T(8,128)(2,1)S(1)}, bf16[128,384]{0,1:T(8,128)(2,1)}, u32[]{:S(2)}, u32[]{:S(2)}) collective-permute-start(bf16[128,384]{0,1:T(8,128)(2,1)S(1)} %get-tuple-element.9), channel_id=1, source_target_pairs={{0,2},{2,4},{4,6},{6,8},{8,10},{10,12},{12,14},{14,16},{16,18},{18... | collective-permute-start | bytes 294920 | tf_op jit(solution)/shard_map/ppermute | solution.py:21
  68.5 7.3 %all_gather.14 = bf16[1024,128]{1,0:T(8,128)(2,1)} all-gather(bf16[512,128]{1,0:T(8,128)(2,1)S(1)} %copy-done.28), channel_id=1, replica_groups=mesh['sp'=16,'tp'=2] {'tp'}, dimensions={0}, use_global_device_ids=true | all-gather | bytes 393216 | tf_op jit(solution)/shard_map/all_gather | solution.py:134
  77.9 3.8 %fusion.164 = f32[1024,256]{0,1:T(8,128)S(1)} fusion(bf16[1024,2048]{1,0:T(8,128)(2,1)} %copy-done.2, bf16[2048,256]{1,0:T(8,128)(2,1)} %param.11), kind=kOutput, calls=%fused_computation.317 | convolution fusion | flops 1073741824 | bytes 6291456 | tf_op jit(solution)/shard_map/dot_general | solution.py:60
  82.1 1.7 %fusion.163 = (f32[4,128]{1,0:T(4,128)}, f32[4,128,384]{1,2,0:T(8,128)}) fusion(bf16[1024,4,32]{0,2,1:T(8,128)(2,1)S(1)} %get-tuple-element.6, bf16[1024,4,32]{0,2,1:T(8,128)(2,1)S(1)} %get-tuple-element.5, bf16[1024,1,32]{0,2,1:T(8,128)(2,1)S(1)} %get-tuple-element.11, bf16[1024,1,32]{0,2,1:T(8,128)(2,1)S(1)} %get-tuple-element.12, ...), kind=kOutput, calls=%fused_computation.316 | convolution fusion | flops 25984512 | bytes 1492992 | tf_op jit(solution)/shard_map/ihd,jd->hij/dot_general | solution.py:92
  84.0 1.8 %fusion.162 = (f32[4,128]{1,0:T(4,128)}, f32[4,128,384]{1,2,0:T(8,128)}) fusion(bf16[1024,4,32]{0,2,1:T(8,128)(2,1)S(1)} %get-tuple-element.6, bf16[1024,4,32]{0,2,1:T(8,128)(2,1)S(1)} %get-tuple-element.5, bf16[1024,1,32]{0,2,1:T(8,128)(2,1)S(1)} %get-tuple-element.11, bf16[1024,1,32]{0,2,1:T(8,128)(2,1)S(1)} %get-tuple-element.12, ...), kind=kOutput, calls=%fused_computation.315 | convolution fusion | flops 25984512 | bytes 1492992 | tf_op jit(solution)/shard_map/ihd,jd->hij/dot_general | solution.py:92
  86.1 1.8 %fusion.161 = (f32[4,128]{1,0:T(4,128)}, f32[4,128,384]{1,2,0:T(8,128)}) fusion(bf16[1024,4,32]{0,2,1:T(8,128)(2,1)S(1)} %get-tuple-element.6, bf16[1024,4,32]{0,2,1:T(8,128)(2,1)S(1)} %get-tuple-element.5, bf16[1024,1,32]{0,2,1:T(8,128)(2,1)S(1)} %get-tuple-element.11, bf16[1024,1,32]{0,2,1:T(8,128)(2,1)S(1)} %get-tuple-element.12, ...), kind=kOutput, calls=%fused_computation.314 | convolution fusion | flops 25984512 | bytes 1492992 | tf_op jit(solution)/shard_map/ihd,jd->hij/dot_general | solution.py:92
  88.1 1.8 %fusion.160 = (f32[4,128]{1,0:T(4,128)}, f32[4,128,384]{1,2,0:T(8,128)}) fusion(bf16[1024,4,32]{0,2,1:T(8,128)(2,1)S(1)} %get-tuple-element.6, bf16[1024,4,32]{0,2,1:T(8,128)(2,1)S(1)} %get-tuple-element.5, bf16[1024,1,32]{0,2,1:T(8,128)(2,1)S(1)} %get-tuple-element.11, bf16[1024,1,32]{0,2,1:T(8,128)(2,1)S(1)} %get-tuple-element.12, ...), kind=kOutput, calls=%fused_computation.313 | convolution fusion | flops 25984512 | bytes 1492992 | tf_op jit(solution)/shard_map/ihd,jd->hij/dot_general | solution.py:92
  90.1 1.8 %fusion.159 = (f32[4,128]{1,0:T(4,128)}, f32[4,128,384]{1,2,0:T(8,128)}) fusion(bf16[1024,4,32]{0,2,1:T(8,128)(2,1)S(1)} %get-tuple-element.6, bf16[1024,4,32]{0,2,1:T(8,128)(2,1)S(1)} %get-tuple-element.5, bf16[1024,1,32]{0,2,1:T(8,128)(2,1)S(1)} %get-tuple-element.11, bf16[1024,1,32]{0,2,1:T(8,128)(2,1)S(1)} %get-tuple-element.12, ...), kind=kOutput, calls=%fused_computation.312 | convolution fusion | flops 25984512 | bytes 1492992 | tf_op jit(solution)/shard_map/ihd,jd->hij/dot_general | solution.py:92
  92.1 1.7 %fusion.158 = (f32[4,128]{1,0:T(4,128)}, f32[4,128,384]{1,2,0:T(8,128)}) fusion(bf16[1024,4,32]{0,2,1:T(8,128)(2,1)S(1)} %get-tuple-element.6, bf16[1024,4,32]{0,2,1:T(8,128)(2,1)S(1)} %get-tuple-element.5, bf16[1024,1,32]{0,2,1:T(8,128)(2,1)S(1)} %get-tuple-element.11, bf16[1024,1,32]{0,2,1:T(8,128)(2,1)S(1)} %get-tuple-element.12, ...), kind=kOutput, calls=%fused_computation.311 | convolution fusion | flops 25984512 | bytes 1492992 | tf_op jit(solution)/shard_map/ihd,jd->hij/dot_general | solution.py:92
  95.8 1.0 fusion.157
  97.8 0.7 exponential_add_fusion
  98.4 1.6 convolution_convert_fusion.3
  100.1 1.6 copy.42
  101.7 1.0 fusion.39
  102.8 1.3 fusion.38
  104.1 1.0 fusion.37
  105.7 0.7 exponential_add_fusion.1
  106.4 0.9 convolution_convert_fusion.4
  107.3 1.6 copy.41
  108.9 1.6 convolution_convert_fusion.5
  110.5 1.6 copy.40
  112.1 2.1 %convolution_convert_fusion.6 = bf16[64,4,128]{2,0,1:T(8,128)(2,1)} fusion(f32[4,128,384]{1,2,0:T(8,128)} %get-tuple-element.42, f32[4,128]{1,0:T(4,128)} %get-tuple-element.29, f32[4,128]{1,0:T(4,128)} %get-tuple-element.20, pred[128,384]{0,1:T(8,128)(4,1)S(1)} %fusion.52, bf16[1024,64]{0,1:T(8,128)(2,1)S(1)} %convolution_convert_fusion.2), kind=kOutput, calls=%fused_computation.41 | convolution fusion | flops 25985024 | bytes 954368 | tf_op jit(solution)/shard_map/hij,jd->ihd/dot_general | solution.py:107
  114.2 1.6 copy.39
  115.8 1.6 convolution_convert_fusion.7
  117.4 1.6 copy.38
  119.0 2.1 %convolution_convert_fusion.8 = bf16[64,4,128]{2,0,1:T(8,128)(2,1)} fusion(f32[4,128,384]{1,2,0:T(8,128)} %get-tuple-element.38, f32[4,128]{1,0:T(4,128)S(1)} %copy-done.58, f32[4,128]{1,0:T(4,128)S(1)} %copy-done.51, pred[128,384]{0,1:T(8,128)(4,1)S(1)} %copy-done.14, bf16[1024,64]{0,1:T(8,128)(2,1)S(1)} %convolution_convert_fusion.2), kind=kOutput, calls=%fused_computation.43 | convolution fusion | flops 25985024 | bytes 954368 | tf_op jit(solution)/shard_map/hij,jd->ihd/dot_general | solution.py:107
  121.1 1.6 copy.37
  122.7 0.9 convolution_convert_fusion.9
  123.6 1.0 copy.36
  124.7 1.1 convolution_convert_fusion.10
  130.9 3.7 %all-to-all-start = ((bf16[2,512,256]{2,1,0:T(8,128)(2,1)}), bf16[2,512,256]{2,1,0:T(8,128)(2,1)S(1)}, u32[]{:S(2)}, u32[]{:S(2)}) async-start(bf16[2,512,256]{2,1,0:T(8,128)(2,1)} %bitcast.49), calls=%async_computation | async-start | bytes 1048576 | tf_op jit(solution)/shard_map/all_to_all | solution.py:130
  134.6 1.1 fusion.42
  137.7 1.6 fusion.22
  139.3 0.8 copy.55
  140.2 2.7 %all-to-all-done = bf16[2,512,256]{2,1,0:T(8,128)(2,1)S(1)} async-done(((bf16[2,512,256]{2,1,0:T(8,128)(2,1)}), bf16[2,512,256]{2,1,0:T(8,128)(2,1)S(1)}, u32[]{:S(2)}, u32[]{:S(2)}) %all-to-all-start) | async-done | bytes 524320 | tf_op jit(solution)/shard_map/all_to_all | solution.py:130
  142.9 3.5 %all-to-all-start.1 = ((bf16[2,512,256]{1,2,0:T(8,128)(2,1)}), bf16[2,512,256]{1,2,0:T(8,128)(2,1)S(1)}, u32[]{:S(2)}, u32[]{:S(2)}) async-start(bf16[2,512,256]{1,2,0:T(8,128)(2,1)} %bitcast.149), calls=%async_computation.1 | async-start | bytes 1048576 | tf_op jit(solution)/shard_map/all_to_all | solution.py:131
  146.6 7.4 %all-to-all-done.1 = bf16[2,512,256]{1,2,0:T(8,128)(2,1)S(1)} async-done(((bf16[2,512,256]{1,2,0:T(8,128)(2,1)}), bf16[2,512,256]{1,2,0:T(8,128)(2,1)S(1)}, u32[]{:S(2)}, u32[]{:S(2)}) %all-to-all-start.1) | async-done | bytes 524320 | tf_op jit(solution)/shard_map/all_to_all | solution.py:131
  154.0 5.9 %convolution_convert_fusion = bf16[512,2048]{1,0:T(8,128)(2,1)} fusion(bf16[1024,2048]{1,0:T(8,128)(2,1)} %all-gather.2.cloned.1.call-done, bf16[512,512]{0,1:T(8,128)(2,1)S(1)} %bitcast.153, bf16[512,512]{0,1:T(8,128)(2,1)S(1)} %bitcast.154), kind=kOutput, calls=%fused_computation.7 | convolution fusion | flops 2150629376 | bytes 7340032 | tf_op jit(solution)/shard_map/dot_general | solution.py:135
  (200 shorter events, 15.1 us)
Async XLA Ops:
  6.5 55.1 %copy-start = (bf16[2048,256]{1,0:T(8,128)(2,1)S(1)}, bf16[2048,256]{1,0:T(8,128)(2,1)}, u32[]{:S(2)}) copy-start(bf16[2048,256]{1,0:T(8,128)(2,1)} %param.14) | copy-start | bytes 3145732
  6.5 147.5 %all-gather.2.cloned.1.call-start = ((), (), s32[]{:S(2)}) async-start(), calls=%async_computation.2 | async-start | bytes 4456448 | tf_op jit(solution)/shard_map/all_gather | solution.py:137
  32.1 3.4 %copy-start.1 = (bf16[1024,2048]{1,0:T(8,128)(2,1)S(1)}, bf16[1024,2048]{1,0:T(8,128)(2,1)}, u32[]{:S(2)}) copy-start(bf16[1024,2048]{1,0:T(8,128)(2,1)} %param.9) | copy-start | bytes 12582916
  35.5 20.2 %copy-start.53 = (f32[2048]{0:T(1024)S(1)}, f32[2048]{0:T(1024)}, u32[]{:S(2)}) copy-start(f32[2048]{0:T(1024)} %param.10) | copy-start | bytes 24580
  58.8 2.8 %copy-start.2 = (bf16[1024,2048]{1,0:T(8,128)(2,1)}, bf16[1024,2048]{1,0:T(8,128)(2,1)S(1)}, u32[]{:S(2)}) copy-start(bf16[1024,2048]{1,0:T(8,128)(2,1)S(1)} %fusion.4) | copy-start | bytes 12582916
  61.6 6.9 %copy-start.28 = (bf16[512,128]{1,0:T(8,128)(2,1)S(1)}, bf16[512,128]{1,0:T(8,128)(2,1)}, u32[]{:S(2)}) copy-start(bf16[512,128]{1,0:T(8,128)(2,1)} %param.17) | copy-start | bytes 393220
  63.6 31.9 %collective-permute-start.1 = (bf16[128,384]{0,1:T(8,128)(2,1)S(1)}, bf16[128,384]{0,1:T(8,128)(2,1)S(1)}, u32[]{:S(2)}, u32[]{:S(2)}) collective-permute-start(bf16[128,384]{0,1:T(8,128)(2,1)S(1)} %get-tuple-element.10), channel_id=1, source_target_pairs={{2,0},{4,2},{6,4},{8,6},{10,8},{12,10},{14,12},{16,14},{18,16},{20... | collective-permute-start | bytes 294920 | tf_op jit(solution)/shard_map/ppermute | solution.py:24
  64.9 31.0 %collective-permute-start = (bf16[128,384]{0,1:T(8,128)(2,1)S(1)}, bf16[128,384]{0,1:T(8,128)(2,1)}, u32[]{:S(2)}, u32[]{:S(2)}) collective-permute-start(bf16[128,384]{0,1:T(8,128)(2,1)S(1)} %get-tuple-element.9), channel_id=1, source_target_pairs={{0,2},{2,4},{4,6},{6,8},{8,10},{10,12},{12,14},{14,16},{16,18},{18... | collective-permute-start | bytes 294920 | tf_op jit(solution)/shard_map/ppermute | solution.py:21
  88.1 5.7 %copy-start.10 = (pred[128,384]{0,1:T(8,128)(4,1)}, pred[128,384]{0,1:T(8,128)(4,1)S(1)}, u32[]{:S(2)}) copy-start(pred[128,384]{0,1:T(8,128)(4,1)S(1)} %fusion.50) | copy-start | bytes 147460
  90.1 5.7 %copy-start.12 = (pred[128,384]{0,1:T(8,128)(4,1)}, pred[128,384]{0,1:T(8,128)(4,1)S(1)}, u32[]{:S(2)}) copy-start(pred[128,384]{0,1:T(8,128)(4,1)S(1)} %fusion.48) | copy-start | bytes 147460
  92.1 4.8 %copy-start.15 = (pred[128,384]{0,1:T(8,128)(4,1)}, pred[128,384]{0,1:T(8,128)(4,1)S(1)}, u32[]{:S(2)}) copy-start(pred[128,384]{0,1:T(8,128)(4,1)S(1)} %fusion.46) | copy-start | bytes 147460
  97.7 4.0 %copy-start.4 = (f32[4,128,384]{1,2,0:T(8,128)S(1)}, f32[4,128,384]{1,2,0:T(8,128)}, u32[]{:S(2)}) copy-start(f32[4,128,384]{1,2,0:T(8,128)} %get-tuple-element.44) | copy-start | bytes 2359300
  101.6 3.4 %copy-start.7 = (f32[4,128,384]{1,2,0:T(8,128)S(1)}, f32[4,128,384]{1,2,0:T(8,128)}, u32[]{:S(2)}) copy-start(f32[4,128,384]{1,2,0:T(8,128)} %get-tuple-element.38) | copy-start | bytes 2359300
  101.6 3.4 %copy-start.13 = (pred[128,384]{0,1:T(8,128)(4,1)S(1)}, pred[128,384]{0,1:T(8,128)(4,1)}, u32[]{:S(2)}) copy-start(pred[128,384]{0,1:T(8,128)(4,1)} %copy-done.12) | copy-start | bytes 147460
  101.7 3.4 %copy-start.50 = (f32[4,128]{1,0:T(4,128)S(1)}, f32[4,128]{1,0:T(4,128)}, u32[]{:S(2)}) copy-start(f32[4,128]{1,0:T(4,128)} %get-tuple-element.18) | copy-start | bytes 6148
  101.7 3.6 %copy-start.8 = (f32[4,128,384]{1,2,0:T(8,128)S(1)}, f32[4,128,384]{1,2,0:T(8,128)}, u32[]{:S(2)}) copy-start(f32[4,128,384]{1,2,0:T(8,128)} %get-tuple-element.36) | copy-start | bytes 2359300
  101.7 3.6 %copy-start.16 = (pred[128,384]{0,1:T(8,128)(4,1)S(1)}, pred[128,384]{0,1:T(8,128)(4,1)}, u32[]{:S(2)}) copy-start(pred[128,384]{0,1:T(8,128)(4,1)} %copy-done.15) | copy-start | bytes 147460
  101.7 3.6 %copy-start.48 = (f32[4,128]{1,0:T(4,128)S(1)}, f32[4,128]{1,0:T(4,128)}, u32[]{:S(2)}) copy-start(f32[4,128]{1,0:T(4,128)} %get-tuple-element.17) | copy-start | bytes 6148
  101.7 3.8 %copy-start.3 = (f32[4,128,384]{1,2,0:T(8,128)S(1)}, f32[4,128,384]{1,2,0:T(8,128)}, u32[]{:S(2)}) copy-start(f32[4,128,384]{1,2,0:T(8,128)} %get-tuple-element.46) | copy-start | bytes 2359300
  101.7 3.8 %copy-start.52 = (f32[4,128]{1,0:T(4,128)S(1)}, f32[4,128]{1,0:T(4,128)}, u32[]{:S(2)}) copy-start(f32[4,128]{1,0:T(4,128)} %get-tuple-element.22) | copy-start | bytes 6148
  102.7 2.9 %copy-start.31 = (f32[4,128]{1,0:T(4,128)S(1)}, f32[4,128]{1,0:T(4,128)}, u32[]{:S(2)}) copy-start(f32[4,128]{1,0:T(4,128)} %get-tuple-element.45) | copy-start | bytes 6148
  102.7 2.9 %copy-start.33 = (f32[4,128]{1,0:T(4,128)S(1)}, f32[4,128]{1,0:T(4,128)}, u32[]{:S(2)}) copy-start(f32[4,128]{1,0:T(4,128)} %get-tuple-element.43) | copy-start | bytes 6148
  102.7 2.9 %copy-start.35 = (f32[4,128]{1,0:T(4,128)S(1)}, f32[4,128]{1,0:T(4,128)}, u32[]{:S(2)}) copy-start(f32[4,128]{1,0:T(4,128)} %get-tuple-element.41) | copy-start | bytes 6148
  102.7 2.9 %copy-start.37 = (f32[4,128]{1,0:T(4,128)S(1)}, f32[4,128]{1,0:T(4,128)}, u32[]{:S(2)}) copy-start(f32[4,128]{1,0:T(4,128)} %get-tuple-element.39) | copy-start | bytes 6148
  102.7 2.9 %copy-start.39 = (f32[4,128]{1,0:T(4,128)S(1)}, f32[4,128]{1,0:T(4,128)}, u32[]{:S(2)}) copy-start(f32[4,128]{1,0:T(4,128)} %get-tuple-element.37) | copy-start | bytes 6148
  102.8 2.9 %copy-start.41 = (f32[4,128]{1,0:T(4,128)S(1)}, f32[4,128]{1,0:T(4,128)}, u32[]{:S(2)}) copy-start(f32[4,128]{1,0:T(4,128)} %get-tuple-element.35) | copy-start | bytes 6148
  102.8 2.9 %copy-start.55 = (f32[4]{0:T(128)S(1)}, f32[4]{0:T(128)}, u32[]{:S(2)}) copy-start(f32[4]{0:T(128)} %param.15) | copy-start | bytes 52
  110.5 5.3 %copy-start.6 = (f32[4,128,384]{1,2,0:T(8,128)S(1)}, f32[4,128,384]{1,2,0:T(8,128)}, u32[]{:S(2)}) copy-start(f32[4,128,384]{1,2,0:T(8,128)} %get-tuple-element.40) | copy-start | bytes 2359300
  110.5 5.3 %copy-start.11 = (pred[128,384]{0,1:T(8,128)(4,1)S(1)}, pred[128,384]{0,1:T(8,128)(4,1)}, u32[]{:S(2)}) copy-start(pred[128,384]{0,1:T(8,128)(4,1)} %copy-done.10) | copy-start | bytes 147460
  114.2 4.8 %copy-start.14 = (pred[128,384]{0,1:T(8,128)(4,1)S(1)}, pred[128,384]{0,1:T(8,128)(4,1)}, u32[]{:S(2)}) copy-start(pred[128,384]{0,1:T(8,128)(4,1)} %copy-done.12) | copy-start | bytes 147460
  114.2 4.8 %copy-start.51 = (f32[4,128]{1,0:T(4,128)S(1)}, f32[4,128]{1,0:T(4,128)}, u32[]{:S(2)}) copy-start(f32[4,128]{1,0:T(4,128)} %get-tuple-element.18) | copy-start | bytes 6148
  114.2 4.8 %copy-start.58 = (f32[4,128]{1,0:T(4,128)S(1)}, f32[4,128]{1,0:T(4,128)}, u32[]{:S(2)}) copy-start(f32[4,128]{1,0:T(4,128)} %get-tuple-element.27) | copy-start | bytes 6148
  117.4 5.3 %copy-start.9 = (f32[4,128,384]{1,2,0:T(8,128)S(1)}, f32[4,128,384]{1,2,0:T(8,128)}, u32[]{:S(2)}) copy-start(f32[4,128,384]{1,2,0:T(8,128)} %get-tuple-element.36) | copy-start | bytes 2359300
  117.4 5.3 %copy-start.17 = (pred[128,384]{0,1:T(8,128)(4,1)S(1)}, pred[128,384]{0,1:T(8,128)(4,1)}, u32[]{:S(2)}) copy-start(pred[128,384]{0,1:T(8,128)(4,1)} %copy-done.15) | copy-start | bytes 147460
  117.4 5.3 %copy-start.49 = (f32[4,128]{1,0:T(4,128)S(1)}, f32[4,128]{1,0:T(4,128)}, u32[]{:S(2)}) copy-start(f32[4,128]{1,0:T(4,128)} %get-tuple-element.17) | copy-start | bytes 6148
  117.4 5.3 %copy-start.57 = (f32[4,128]{1,0:T(4,128)S(1)}, f32[4,128]{1,0:T(4,128)}, u32[]{:S(2)}) copy-start(f32[4,128]{1,0:T(4,128)} %get-tuple-element.26) | copy-start | bytes 6148
  121.1 3.5 %copy-start.19 = (pred[128,384]{0,1:T(8,128)(4,1)S(1)}, pred[128,384]{0,1:T(8,128)(4,1)}, u32[]{:S(2)}) copy-start(pred[128,384]{0,1:T(8,128)(4,1)} %copy-done.18) | copy-start | bytes 147460
  121.1 3.5 %copy-start.47 = (f32[4,128]{1,0:T(4,128)S(1)}, f32[4,128]{1,0:T(4,128)}, u32[]{:S(2)}) copy-start(f32[4,128]{1,0:T(4,128)} %copy-done.46) | copy-start | bytes 6148
  121.1 3.5 %copy-start.56 = (f32[4,128]{1,0:T(4,128)S(1)}, f32[4,128]{1,0:T(4,128)}, u32[]{:S(2)}) copy-start(f32[4,128]{1,0:T(4,128)} %get-tuple-element.16) | copy-start | bytes 6148
  123.6 3.5 %copy-start.27 = (bf16[128,256]{1,0:T(8,128)(2,1)S(1)}, bf16[128,256]{1,0:T(8,128)(2,1)}, u32[]{:S(2)}) copy-start(bf16[128,256]{1,0:T(8,128)(2,1)} %copy.37) | copy-start | bytes 196612
  124.6 3.2 %copy-start.26 = (bf16[128,256]{1,0:T(8,128)(2,1)S(1)}, bf16[128,256]{1,0:T(8,128)(2,1)}, u32[]{:S(2)}) copy-start(bf16[128,256]{1,0:T(8,128)(2,1)} %copy.38) | copy-start | bytes 196612
  124.6 3.8 %copy-start.25 = (bf16[128,256]{1,0:T(8,128)(2,1)S(1)}, bf16[128,256]{1,0:T(8,128)(2,1)}, u32[]{:S(2)}) copy-start(bf16[128,256]{1,0:T(8,128)(2,1)} %copy.39) | copy-start | bytes 196612
  124.6 4.4 %copy-start.24 = (bf16[128,256]{1,0:T(8,128)(2,1)S(1)}, bf16[128,256]{1,0:T(8,128)(2,1)}, u32[]{:S(2)}) copy-start(bf16[128,256]{1,0:T(8,128)(2,1)} %copy.40) | copy-start | bytes 196612
  124.7 5.0 %copy-start.23 = (bf16[128,256]{1,0:T(8,128)(2,1)S(1)}, bf16[128,256]{1,0:T(8,128)(2,1)}, u32[]{:S(2)}) copy-start(bf16[128,256]{1,0:T(8,128)(2,1)} %copy.41) | copy-start | bytes 196612
  124.7 5.6 %copy-start.22 = (bf16[128,256]{1,0:T(8,128)(2,1)S(1)}, bf16[128,256]{1,0:T(8,128)(2,1)}, u32[]{:S(2)}) copy-start(bf16[128,256]{1,0:T(8,128)(2,1)} %copy.42) | copy-start | bytes 196612
  124.7 9.9 %copy-start.21 = (bf16[128,384]{0,1:T(8,128)(2,1)S(1)}, bf16[128,384]{0,1:T(8,128)(2,1)}, u32[]{:S(2)}) copy-start(bf16[128,384]{0,1:T(8,128)(2,1)} %copy-done.20) | copy-start | bytes 294916
  130.9 12.0 %all-to-all-start = ((bf16[2,512,256]{2,1,0:T(8,128)(2,1)}), bf16[2,512,256]{2,1,0:T(8,128)(2,1)S(1)}, u32[]{:S(2)}, u32[]{:S(2)}) async-start(bf16[2,512,256]{2,1,0:T(8,128)(2,1)} %bitcast.49), calls=%async_computation | async-start | bytes 1048576 | tf_op jit(solution)/shard_map/all_to_all | solution.py:130
  142.9 11.1 %all-to-all-start.1 = ((bf16[2,512,256]{1,2,0:T(8,128)(2,1)}), bf16[2,512,256]{1,2,0:T(8,128)(2,1)S(1)}, u32[]{:S(2)}, u32[]{:S(2)}) async-start(bf16[2,512,256]{1,2,0:T(8,128)(2,1)} %bitcast.149), calls=%async_computation.1 | async-start | bytes 1048576 | tf_op jit(solution)/shard_map/all_to_all | solution.py:131
  (21 other events, 26.9 us)
Sparse Core Ops, SparseCore 0:
  76.0 49.8 all-gather.1
where the time goes:
time: 168 us; the launch traced here: 167 us
  blocking collectives  50.8 us (30%)
  matrix products  37.6 us (22%)
  other arithmetic  22.2 us (13%)
  local copies, waits for them, and re-layouts  19.4 us (12%)
  between operations  14.5 us (9%)
  starting transfers between devices  12.2 us (7%)
  waiting for transfers between devices  10.2 us (6%)
    all_gather x1, blocking collectives, body(): lax.all_gather(key_cols, 'sp', axis=0, tiled=True)  24.6 us
    all_gather x1, blocking collectives, body(): lax.all_gather(value_cols, 'sp', axis=0, tiled=True)  18.9 us
    dot_general x8, matrix products, body(): jnp.einsum('hij,jd->ihd', weights, values, preferred_element_type=jnp.flo...  11.9 us
    dot_general x8, matrix products, body(): jnp.einsum('ihd,jd->hij', queries, keys, preferred_element_type=jnp.float32)  11.9 us
    convert_element_type x8, local copies, waits for them, and re-layouts, body(): results.append(result.reshape(QB, local_heads * HEAD).astype(jnp.bfloat16))  10.6 us
    all_to_all x1, waiting for transfers between devices, body(): lax.all_to_all(pooled, 'tp', split_axis=0, concat_axis=1, tiled=True)  7.42 us
    all_gather x1, blocking collectives, body(): out_rows_all = lax.all_gather(w_out, 'tp', axis=0, tiled=True)  7.31 us
    dot_general x1, matrix products, body(): jnp.dot(joined, lax.all_gather(out_rows_all, 'sp', axis=1, tiled=True), p...  5.88 us
  transfers between devices with their start and end apart: 5, of which 2 were waited for; matrix products, arithmetic and copies ran while one was open for 35% of the time, Pallas kernels for 0%

commit v1 on v0

--- a/solution.py
+++ b/solution.py
@@ -11,6 +11,12 @@
 QB = 128
 NEG_BIG = -1e30
 POOL_SPANS = (2, 4, 8, 16)
+
+
+def trade_parts(shard, axis, split, join):
+    parts = jnp.split(shard, lax.axis_size(axis), axis=split)
+    incoming = lax.all_to_all(jnp.stack(parts), axis, 0, 0)
+    return jnp.concatenate(incoming, axis=join)
 
 
 def extended(block, sides, width):
@@ -128,7 +134,7 @@
     pooled = ((measured - pool_vals[reach : reach + local_rows]) * pool_scale).astype(jnp.bfloat16)
     attended_rows, pooled_rows = (
         lax.all_to_all(attended, "tp", split_axis=0, concat_axis=1, tiled=True),
-        lax.all_to_all(pooled, "tp", split_axis=0, concat_axis=1, tiled=True),
+        trade_parts(pooled, "tp", 0, 1),
     )
     joined = jnp.concatenate([attended_rows, pooled_rows], axis=1)
     out_rows_all = lax.all_gather(w_out, "tp", axis=0, tiled=True)

time: 168 us -> 146 us (0.87)
  local copies, waits for them, and re-layouts: 19.4 us -> 4.6 us
  matrix products: 37.6 us -> 26 us
  blocking collectives: 50.8 us -> 60.9 us
  waiting for transfers between devices: 10.2 us -> 3.73 us
  other arithmetic: 22.2 us -> 27.1 us
  starting transfers between devices: 12.2 us -> 8.44 us
    convert_element_type x8 -> x0, local copies, waits for them, and re-layouts: 10.6 us -> none  [body(): results.append(result.reshape(QB, local_heads * HEAD).astype(jnp.bfloat16))]
    all_to_all x0 -> x1, blocking collectives: none -> 10.2 us  [trade_parts(): incoming = lax.all_to_all(jnp.stack(parts), axis, 0, 0)]
    dot_general x8, matrix products: 11.9 us -> 4.02 us  [body(): jnp.einsum('hij,jd->ihd', weights, values, preferred_element_type=jnp.flo...]
    all_to_all x1 -> x0, waiting for transfers between devices: 7.42 us -> none  [body(): lax.all_to_all(pooled, 'tp', split_axis=0, concat_axis=1, tiled=True)]
    dot_general x8, matrix products: 11.9 us -> 8.27 us  [body(): jnp.einsum('ihd,jd->hij', queries, keys, preferred_element_type=jnp.float32)]
    all_to_all x1 -> x0, starting transfers between devices: 3.49 us -> none  [body(): lax.all_to_all(pooled, 'tp', split_axis=0, concat_axis=1, tiled=True)]
    lt x8, other arithmetic: 0.06 us -> 3.48 us  [body(): key_pos[None, :] < seq_total]
    unnamed x135 -> x73, local copies, waits for them, and re-layouts: 5.75 us -> 2.33 us
  transfers between devices with their start and end apart: 5 -> 4, of which waited for: 2 -> 1; matrix products, arithmetic and copies ran while one was open for 35% -> 25% of each run, Pallas kernels for 0% -> 0%
where the time goes in v1:
time: 146 us; the launch traced here: 145 us
  blocking collectives  60.9 us (42%)
  other arithmetic  27.1 us (19%)
  matrix products  26 us (18%)
  between operations  14.1 us (10%)
  starting transfers between devices  8.44 us (6%)
  local copies, waits for them, and re-layouts  4.6 us (3%)
  waiting for transfers between devices  3.73 us (3%)
    all_gather x1, blocking collectives, body(): lax.all_gather(key_cols, 'sp', axis=0, tiled=True)  24.6 us
    all_gather x1, blocking collectives, body(): lax.all_gather(value_cols, 'sp', axis=0, tiled=True)  18.9 us
    all_to_all x1, blocking collectives, trade_parts(): incoming = lax.all_to_all(jnp.stack(parts), axis, 0, 0)  10.2 us
    dot_general x8, matrix products, body(): jnp.einsum('ihd,jd->hij', queries, keys, preferred_element_type=jnp.float32)  8.27 us
    all_gather x1, blocking collectives, body(): out_rows_all = lax.all_gather(w_out, 'tp', axis=0, tiled=True)  7.31 us
    dot_general x1, matrix products, body(): jnp.dot(joined, lax.all_gather(out_rows_all, 'sp', axis=1, tiled=True), p...  5.88 us
    dot_general x8, matrix products, body(): jnp.einsum('hij,jd->ihd', weights, values, preferred_element_type=jnp.flo...  4.02 us
    dot_general x1, matrix products, body(): jnp.dot(normed, w_query, preferred_element_type=jnp.float32)  3.78 us
  transfers between devices with their start and end apart: 4, of which 1 were waited for; matrix products, arithmetic and copies ran while one was open for 25% of the time, Pallas kernels for 0%

profile of v1, /device:TPU:0, one launch (start us, length us, event | category | flops | bytes accessed | tf_op | source)
XLA Modules:
  0.0 144.9 jit_solution(8550265951908007729)
XLA Ops:
  6.6 0.9 constant_dynamic-slice_fusion.1
  7.5 24.6 %all_gather.12 = bf16[2048,64]{1,0:T(8,128)(2,1)S(1)} all-gather(bf16[128,64]{1,0:T(8,128)(2,1)S(1)} %constant_dynamic-slice_fusion.1), channel_id=1, replica_groups=mesh['sp'=16,'tp'=2] {'sp'}, dimensions={0}, use_global_device_ids=true | all-gather | bytes 278528 | tf_op jit(solution)/shard_map/all_gather | solution.py:76
  32.1 3.0 %convert_reduce_fusion = f32[1024]{0:T(1024)S(1)} fusion(bf16[1024,2048]{1,0:T(8,128)(2,1)} %param.9), kind=kLoop, calls=%fused_computation.1 | loop fusion | flops 4193280 | bytes 4198400 | tf_op jit(solution)/shard_map/reduce_sum | solution.py:37
  35.5 1.2 fusion.2
  36.9 18.9 %all_gather.13 = bf16[2048,64]{1,0:T(8,128)(2,1)S(1)} all-gather(bf16[128,64]{1,0:T(8,128)(2,1)S(1)} %constant_dynamic-slice_fusion), channel_id=1, replica_groups=mesh['sp'=16,'tp'=2] {'sp'}, dimensions={0}, use_global_device_ids=true | all-gather | bytes 278528 | tf_op jit(solution)/shard_map/all_gather | solution.py:81
  55.8 3.0 %fusion.4 = bf16[1024,2048]{1,0:T(8,128)(2,1)S(1)} fusion(bf16[1024,2048]{1,0:T(8,128)(2,1)} %param.9, f32[2048]{0:T(1024)S(1)} %copy-done.14, f32[1024]{0:T(1024)S(1)} %add_rsqrt_fusion, f32[1024]{0:T(1024)S(1)} %broadcast_multiply_fusion), kind=kLoop, calls=%fused_computation.6 | loop fusion | flops 10485760 | bytes 8404992 | tf_op jit(solution)/shard_map/convert_element_type | solution.py:39
  58.8 1.4 convolution_bitcast_fusion
  60.2 1.4 convolution_convert_fusion.2
  61.6 1.3 convolution_convert_fusion.1
  62.9 0.6 fusion.64
  63.5 0.7 pad_maximum_fusion.8
  64.2 1.3 collective-permute-start.1
  65.5 3.7 %collective-permute-start = (bf16[128,384]{0,1:T(8,128)(2,1)}, bf16[128,384]{0,1:T(8,128)(2,1)}, u32[]{:S(2)}, u32[]{:S(2)}) collective-permute-start(bf16[128,384]{0,1:T(8,128)(2,1)} %get-tuple-element.9), channel_id=1, source_target_pairs={{0,2},{2,4},{4,6},{6,8},{8,10},{10,12},{12,14},{14,16},{16,18},{18... | collective-permute-start | bytes 294920 | tf_op jit(solution)/shard_map/ppermute | solution.py:27
  69.2 7.3 %all_gather.14 = bf16[1024,128]{1,0:T(8,128)(2,1)} all-gather(bf16[512,128]{1,0:T(8,128)(2,1)S(1)} %copy-done.10), channel_id=1, replica_groups=mesh['sp'=16,'tp'=2] {'tp'}, dimensions={0}, use_global_device_ids=true | all-gather | bytes 393216 | tf_op jit(solution)/shard_map/all_gather | solution.py:140
  77.6 0.6 iota_add_fusion.11
  78.2 0.6 fusion.128
  79.4 0.6 fusion.124
  79.9 0.6 iota_add_fusion.14
  81.0 0.6 fusion.122
  81.6 0.6 fusion.134
  82.2 0.6 iota_add_fusion.1
  82.8 0.6 fusion.120
  83.4 0.6 iota_add_fusion.8
  84.0 0.6 iota_add_fusion.16
  84.6 0.6 subtract_convert_fusion.3
  85.2 3.8 %fusion.164 = f32[1024,256]{0,1:T(8,128)S(1)} fusion(bf16[1024,2048]{1,0:T(8,128)(2,1)} %copy-done.2, bf16[2048,256]{1,0:T(8,128)(2,1)} %param.11), kind=kOutput, calls=%fused_computation.320 | convolution fusion | flops 1073741824 | bytes 6291456 | tf_op jit(solution)/shard_map/dot_general | solution.py:66
  90.0 1.2 fusion.162
  91.4 1.2 fusion.161
  92.9 1.2 fusion.160
  94.3 1.2 fusion.159
  95.7 0.6 copy-done.8
  96.3 1.2 fusion.158
  97.5 0.6 broadcast_compare_fusion
  98.1 0.9 fusion.58
  99.0 0.9 fusion.44
  99.9 0.6 broadcast_compare_fusion.2
  100.5 1.0 fusion.156
  101.5 1.0 fusion.157
  103.0 1.2 convolution_convert_fusion.10
  104.8 0.7 copy-done.6
  108.1 1.0 convolution_convert_fusion.3
  109.2 0.8 copy.29
  110.0 3.5 %all-to-all-start = ((bf16[2,512,256]{1,2,0:T(8,128)(2,1)}), bf16[2,512,256]{1,2,0:T(8,128)(2,1)S(1)}, u32[]{:S(2)}, u32[]{:S(2)}) async-start(bf16[2,512,256]{1,2,0:T(8,128)(2,1)} %bitcast.153), calls=%async_computation | async-start | bytes 1048576 | tf_op jit(solution)/shard_map/all_to_all | solution.py:136
  113.5 1.1 fusion.42
  116.5 1.6 %fusion.22 = bf16[1024,256]{0,1:T(8,128)(2,1)S(1)} fusion(f32[1040,256]{0,1:T(8,128)S(1)} %fusion.42, f32[1025,256]{0,1:T(8,128)S(1)} %get-tuple-element.8, f32[1025,256]{0,1:T(8,128)S(1)} %get-tuple-element.7, f32[1033,256]{0,1:T(8,128)S(1)} %slice_add_fusion, f32[1037,256]{0,1:T(8,128)S(1)} %slice_add_fusion.1, f32[1039,256]{0,1:T(8,128)S(1)} %slice_add_fusion.2, ...), kind=kLoop, calls=%fused_computation.48 | loop fusion | flops 3932160 | bytes 6834176 | tf_op jit(solution)/shard_map/convert_element_type | solution.py:134
  118.3 3.7 %all-to-all-done = bf16[2,512,256]{1,2,0:T(8,128)(2,1)S(1)} async-done(((bf16[2,512,256]{1,2,0:T(8,128)(2,1)}), bf16[2,512,256]{1,2,0:T(8,128)(2,1)S(1)}, u32[]{:S(2)}, u32[]{:S(2)}) %all-to-all-start) | async-done | bytes 524320 | tf_op jit(solution)/shard_map/all_to_all | solution.py:136
  122.0 10.2 %all_to_all.24 = bf16[2,512,256]{1,2,0:T(8,128)(2,1)S(1)} all-to-all(bf16[2,512,256]{1,2,0:T(8,128)(2,1)S(1)} %pad_maximum_fusion.4), channel_id=1, replica_groups=mesh['sp'=16,'tp'=2] {'tp'}, dimensions={0} | all-to-all | bytes 1048576 | tf_op jit(solution)/shard_map/all_to_all | solution.py:18
  132.2 5.9 %convolution_convert_fusion = bf16[512,2048]{1,0:T(8,128)(2,1)} fusion(bf16[1024,2048]{1,0:T(8,128)(2,1)} %all-gather.2.cloned.1.call-done, bf16[512,512]{0,1:T(8,128)(2,1)S(1)} %bitcast.157, bf16[512,512]{0,1:T(8,128)(2,1)S(1)} %bitcast.156), kind=kOutput, calls=%fused_computation.7 | convolution fusion | flops 2150629376 | bytes 7340032 | tf_op jit(solution)/shard_map/dot_general | solution.py:141
  (130 shorter events, 10.1 us)
Async XLA Ops:
  6.5 55.1 %copy-start = (bf16[2048,256]{1,0:T(8,128)(2,1)S(1)}, bf16[2048,256]{1,0:T(8,128)(2,1)}, u32[]{:S(2)}) copy-start(bf16[2048,256]{1,0:T(8,128)(2,1)} %param.14) | copy-start | bytes 3145732
  6.5 125.7 %all-gather.2.cloned.1.call-start = ((), (), s32[]{:S(2)}) async-start(), calls=%async_computation.2 | async-start | bytes 4456448 | tf_op jit(solution)/shard_map/all_gather | solution.py:143
  32.1 3.4 %copy-start.1 = (bf16[1024,2048]{1,0:T(8,128)(2,1)S(1)}, bf16[1024,2048]{1,0:T(8,128)(2,1)}, u32[]{:S(2)}) copy-start(bf16[1024,2048]{1,0:T(8,128)(2,1)} %param.9) | copy-start | bytes 12582916
  35.5 1.3 copy-start.11
  35.5 20.2 %copy-start.14 = (f32[2048]{0:T(1024)S(1)}, f32[2048]{0:T(1024)}, u32[]{:S(2)}) copy-start(f32[2048]{0:T(1024)} %param.10) | copy-start | bytes 24580
  58.8 2.8 %copy-start.2 = (bf16[1024,2048]{1,0:T(8,128)(2,1)}, bf16[1024,2048]{1,0:T(8,128)(2,1)S(1)}, u32[]{:S(2)}) copy-start(bf16[1024,2048]{1,0:T(8,128)(2,1)S(1)} %fusion.4) | copy-start | bytes 12582916
  61.6 7.6 %copy-start.10 = (bf16[512,128]{1,0:T(8,128)(2,1)S(1)}, bf16[512,128]{1,0:T(8,128)(2,1)}, u32[]{:S(2)}) copy-start(bf16[512,128]{1,0:T(8,128)(2,1)} %param.17) | copy-start | bytes 393220
  64.2 36.2 %collective-permute-start.1 = (bf16[128,384]{0,1:T(8,128)(2,1)}, bf16[128,384]{0,1:T(8,128)(2,1)}, u32[]{:S(2)}, u32[]{:S(2)}) collective-permute-start(bf16[128,384]{0,1:T(8,128)(2,1)} %get-tuple-element.10), channel_id=1, source_target_pairs={{2,0},{4,2},{6,4},{8,6},{10,8},{12,10},{14,12},{16,14},{18,16},{20... | collective-permute-start | bytes 294920 | tf_op jit(solution)/shard_map/ppermute | solution.py:30
  65.5 35.9 %collective-permute-start = (bf16[128,384]{0,1:T(8,128)(2,1)}, bf16[128,384]{0,1:T(8,128)(2,1)}, u32[]{:S(2)}, u32[]{:S(2)}) collective-permute-start(bf16[128,384]{0,1:T(8,128)(2,1)} %get-tuple-element.9), channel_id=1, source_target_pairs={{0,2},{2,4},{4,6},{6,8},{8,10},{10,12},{12,14},{14,16},{16,18},{18... | collective-permute-start | bytes 294920 | tf_op jit(solution)/shard_map/ppermute | solution.py:27
  89.0 0.7 copy-start.26
  89.0 0.7 copy-start.27
  89.0 0.7 copy-start.28
  89.0 2.2 %copy-start.23 = (pred[384]{0:T(512)(128)(4,1)S(1)}, pred[384]{0:T(512)(128)(4,1)}, u32[]{:S(2)}) copy-start(pred[384]{0:T(512)(128)(4,1)} %get-tuple-element.67) | copy-start | bytes 1156
  89.0 2.2 %copy-start.24 = (pred[384]{0:T(512)(128)(4,1)S(1)}, pred[384]{0:T(512)(128)(4,1)}, u32[]{:S(2)}) copy-start(pred[384]{0:T(512)(128)(4,1)} %get-tuple-element.68) | copy-start | bytes 1156
  89.0 2.2 %copy-start.25 = (s32[128]{0:T(128)S(1)}, s32[128]{0:T(128)}, u32[]{:S(2)}) copy-start(s32[128]{0:T(128)} %iota_add_fusion.12) | copy-start | bytes 1540
  90.0 4.1 %copy-start.20 = (pred[384]{0:T(512)(128)(4,1)S(1)}, pred[384]{0:T(512)(128)(4,1)}, u32[]{:S(2)}) copy-start(pred[384]{0:T(512)(128)(4,1)} %get-tuple-element.63) | copy-start | bytes 1156
  90.0 4.1 %copy-start.21 = (pred[384]{0:T(512)(128)(4,1)S(1)}, pred[384]{0:T(512)(128)(4,1)}, u32[]{:S(2)}) copy-start(pred[384]{0:T(512)(128)(4,1)} %get-tuple-element.64) | copy-start | bytes 1156
  90.0 4.1 %copy-start.22 = (s32[128]{0:T(128)S(1)}, s32[128]{0:T(128)}, u32[]{:S(2)}) copy-start(s32[128]{0:T(128)} %iota_add_fusion.14) | copy-start | bytes 1540
  91.4 4.1 %copy-start.17 = (s32[128]{0:T(128)S(1)}, s32[128]{0:T(128)}, u32[]{:S(2)}) copy-start(s32[128]{0:T(128)} %iota_add_fusion.15) | copy-start | bytes 1540
  91.4 4.1 %copy-start.18 = (pred[384]{0:T(512)(128)(4,1)S(1)}, pred[384]{0:T(512)(128)(4,1)}, u32[]{:S(2)}) copy-start(pred[384]{0:T(512)(128)(4,1)} %get-tuple-element.53) | copy-start | bytes 1156
  91.4 4.1 %copy-start.19 = (pred[384]{0:T(512)(128)(4,1)S(1)}, pred[384]{0:T(512)(128)(4,1)}, u32[]{:S(2)}) copy-start(pred[384]{0:T(512)(128)(4,1)} %get-tuple-element.54) | copy-start | bytes 1156
  95.7 0.6 copy-start.8
  100.4 2.1 %copy-start.15 = (f32[4]{0:T(128)S(1)}, f32[4]{0:T(128)}, u32[]{:S(2)}) copy-start(f32[4]{0:T(128)} %param.15) | copy-start | bytes 52
  102.9 1.3 copy-start.3
  103.0 1.4 copy-start.4
  103.0 1.6 %copy-start.5 = (f32[4,128,384]{1,2,0:T(8,128)S(1)}, f32[4,128,384]{1,2,0:T(8,128)}, u32[]{:S(2)}) copy-start(f32[4,128,384]{1,2,0:T(8,128)} %get-tuple-element.42) | copy-start | bytes 2359300
  104.2 1.2 copy-start.6
  104.2 1.5 %copy-start.7 = (f32[4,128,384]{1,2,0:T(8,128)S(1)}, f32[4,128,384]{1,2,0:T(8,128)}, u32[]{:S(2)}) copy-start(f32[4,128,384]{1,2,0:T(8,128)} %get-tuple-element.38) | copy-start | bytes 2359300
  104.2 1.4 copy-start.9
  110.0 12.0 %all-to-all-start = ((bf16[2,512,256]{1,2,0:T(8,128)(2,1)}), bf16[2,512,256]{1,2,0:T(8,128)(2,1)S(1)}, u32[]{:S(2)}, u32[]{:S(2)}) async-start(bf16[2,512,256]{1,2,0:T(8,128)(2,1)} %bitcast.153), calls=%async_computation | async-start | bytes 1048576 | tf_op jit(solution)/shard_map/all_to_all | solution.py:136
  115.8 0.7 copy-start.12
  115.8 0.7 copy-start.13
  115.8 0.7 copy-start.16
  115.9 0.7 copy-start.29
  115.9 0.7 copy-start.30
  115.9 0.7 copy-start.31
  115.9 0.7 copy-start.32
Sparse Core Ops, SparseCore 0:
  76.7 50.9 all-gather.1
